TPU v7x, 32 devices: a whole 2x2x4 slice. The times are simulated.
32 devices in a mesh: ra: 16 (over z, y, x), cb: 2 (over core).
Axes of the slice: x: 2, y: 2, z: 4, core: 2. Of those that a mesh axis runs over, the one named last changes fastest.
Arguments:
- activations: bfloat16 [768, 4096], P('ra', 'cb'), may hold values from -230 to 230
- gain_first: float32 [4096], P('cb'), may hold values from 0.1 to 1.9
- gate_weight: float32 [11264, 4096], P('ra', 'cb'), may hold values from -0.125 to 0.125
- gate_scale: float32 [11264], P('ra'), may hold values from 0.5 to 2
- up_weight: float32 [11264, 4096], P('ra', 'cb'), may hold values from -0.125 to 0.125
- up_scale: float32 [11264], P('ra'), may hold values from 0.5 to 2
- down_weight: float32 [11264, 4096], P('ra', 'cb'), may hold values from -0.0546875 to 0.0546875
- down_scale: float32 [4096], P('cb'), may hold values from 0.35 to 2.8
- gain_second: float32 [4096], P('cb'), may hold values from 0.1 to 1.9
Outputs:
- normed: bfloat16 [768, 4096], P('ra', 'cb')
All inputs are finite; a program needn't handle non-finite values.
Results may differ from a plain program's by a relative error of at most 0.011.
Values may be sent and summed in bfloat16 or wider, within the bound.
A program may use at most 64 MiB of HBM per device.

v0:
```python
import functools

import jax
import jax.numpy as jnp
from jax import lax
from jax.experimental import pallas as pl
from jax.experimental.pallas import tpu as pltpu
from jax.sharding import PartitionSpec as P

EPS = 1e-06
MESH = pl.DeviceIdType.MESH
F32 = jnp.float32
BF16 = jnp.bfloat16


def flip(index, mask):
    bit = 1
    while bit <= mask:
        if mask & bit:
            index = index + (1 - 2 * ((index // bit) % 2)) * bit
        bit *= 2
    return index


def kernel(
    planes,
    features,
    x_ref,
    gain_ref,
    gate_hbm,
    gate_scale_ref,
    up_hbm,
    up_scale_ref,
    down_hbm,
    down_scale_ref,
    gain2_ref,
    out_ref,
    wide,
    gate_w,
    up_w,
    down_w,
    xg,
    scaled,
    hidden,
    part,
    ex_send,
    ex_recv,
    sq_send,
    sq_recv,
    keep_a,
    keep_b,
    send_a,
    send_b,
    recv_a,
    recv_b,
    send2_a,
    send2_b,
    recv2_a,
    recv2_b,
    own_sum,
    z_send,
    z_recv,
    last_send,
    last_recv,
    w_sem,
    ssem,
    rsem,
):
    ra = lax.axis_index("ra")
    cb = lax.axis_index("cb")
    rows, width = x_ref.shape
    half = width // 2
    x_peer = (flip(ra, 1), cb)
    y_peer = (flip(ra, 2), cb)
    z_peers = [None] + [(flip(ra, 4 * k), cb) for k in range(1, planes)]
    core_peer = (ra, flip(cb, 1))
    first, second = pl.ds(0, half), pl.ds(half, half)

    loads = []
    for i, src in enumerate((gate_hbm, up_hbm, down_hbm)):
        load = pltpu.make_async_copy(src, wide.at[i], w_sem.at[i])
        load.start()
        loads.append(load)

    barrier = pltpu.get_barrier_semaphore()
    peers = [x_peer, y_peer, core_peer] + z_peers[1:]
    for peer in peers:
        pl.semaphore_signal(barrier, inc=1, device_id=peer, device_id_type=MESH)
    pl.semaphore_wait(barrier, len(peers))

    copies = {}

    def send(name, k, src, dst, peer):
        slot = len(copies)
        copy = pltpu.make_async_remote_copy(
            src_ref=src,
            dst_ref=dst,
            send_sem=ssem.at[slot],
            recv_sem=rsem.at[slot],
            device_id=peer,
            device_id_type=MESH,
        )
        copy.start()
        copies[name, k] = copy

    def arrived(name, k):
        copies[name, k].wait_recv()

    halves = (first, second)

    def spread(k):
        for i in (1, 0):
            if k:
                arrived(("z", i), k)
            for name, slot, peer in (("gx", 1, x_peer), ("gy", 2, y_peer)):
                h = i if k or name == "gx" else 1 - i
                src = (xg.at[k, 0] if k else x_ref).at[:, halves[h]]
                send((name, h), k, src, xg.at[k, slot, :, halves[h]], peer)

    def forward(k):
        arrived(("gx", 1), k)
        send("fy", k, xg.at[k, 1, :, second], xg.at[k, 3, :, second], y_peer)
        arrived(("gy", 0), k)
        send("fx", k, xg.at[k, 2, :, first], xg.at[k, 3, :, first], x_peer)

    nt = (((1,), (1,)), ((), ()))

    def gate_up(k):
        arrived(("gx", 0), k)
        arrived(("gy", 1), k)
        arrived("fx", k)
        arrived("fy", k)

        def prepare(s, carry):
            block = xg[k, s].astype(F32)
            squares = jnp.sum(block * block, axis=1, keepdims=True)
            sq_send[k, s] = jnp.broadcast_to(squares, (rows, 128))
            scaled[s] = (block * gain_ref[...]).astype(BF16)
            return carry

        lax.fori_loop(0, 4, prepare, 0)
        send("sq", k, sq_send.at[k], sq_recv.at[k], core_peer)
        tokens = scaled[...].reshape(4 * rows, width)
        for i, w in enumerate((gate_w, up_w)):
            product = lax.dot_general(tokens, w[...], nt, preferred_element_type=F32)
            part[k, i] = product
            ex_send[k, i] = product.astype(BF16)
            send(("ex", i), k, ex_send.at[k, i], ex_recv.at[k, i], core_peer)

    def down(k):
        arrived("sq", k)
        arrived(("ex", 0), k)
        arrived(("ex", 1), k)

        for s in range(4):
            here = slice(s * rows, (s + 1) * rows)
            squares = (sq_send[k, s] + sq_recv[k, s])[:, :1]
            rscale = lax.rsqrt(squares / features + EPS)
            gate = (part[k, 0, here] + ex_recv[k, 0, here].astype(F32)) * rscale * gate_scale_ref[...][None, :]
            up = (part[k, 1, here] + ex_recv[k, 1, here].astype(F32)) * rscale * up_scale_ref[...][None, :]
            hidden[here] = (gate / (1.0 + jnp.exp(-gate)) * up).astype(BF16)
        units = hidden[...]
        prod = jnp.dot(units, down_w[:, :half], preferred_element_type=F32)
        for dy in range(2):
            low = 2 * dy * rows
            keep_a[k, dy] = prod[low : low + rows]
            send_a[k, dy] = prod[low + rows : low + 2 * rows].astype(BF16)
        prod = jnp.dot(units, down_w[:, half:], preferred_element_type=F32)
        for dx in range(2):
            low = dx * rows
            keep_b[k, dx] = prod[low : low + rows]
            low += 2 * rows
            send_b[k, dx] = prod[low : low + rows].astype(BF16)

    def issue(k):
        send("a1", k, send_a.at[k], recv_a.at[k], x_peer)
        send("b1", k, send_b.at[k], recv_b.at[k], y_peer)

    def reduce_one(k):
        arrived("a1", k)
        send2_a[k] = (keep_a[k, 1] + recv_a[k, 1].astype(F32)).astype(BF16)
        send("a2", k, send2_a.at[k], recv2_a.at[k], y_peer)
        arrived("b1", k)
        send2_b[k] = (keep_b[k, 1] + recv_b[k, 1].astype(F32)).astype(BF16)
        send("b2", k, send2_b.at[k], recv2_b.at[k], x_peer)

    def reduce_two(k):
        arrived("a2", k)
        sum_a = keep_a[k, 0] + recv_a[k, 0].astype(F32) + recv2_a[k].astype(F32)
        arrived("b2", k)
        sum_b = keep_b[k, 0] + recv_b[k, 0].astype(F32) + recv2_b[k].astype(F32)
        if k == 0:
            own_sum[:, :half] = sum_a
            own_sum[:, half:] = sum_b
        else:
            z_send[k, :, :half] = sum_a.astype(BF16)
            z_send[k, :, half:] = sum_b.astype(BF16)
            send("zs", k, z_send.at[k], z_recv.at[k], z_peers[k])

    def narrow(i, target):
        loads[i].wait()
        step = 64

        def body(j, carry):
            here = pl.ds(pl.multiple_of(j * step, step), step)
            target[here] = wide[i, here].astype(BF16)
            return carry

        lax.fori_loop(0, target.shape[0] // step, body, 0)

    spread(0)
    for k in range(1, planes):
        for i in (1, 0):
            part_of = pl.ds(i * half, half)
            send(("z", i), k, x_ref.at[:, part_of], xg.at[k, 0, :, part_of], z_peers[k])
    xg[0, 0] = x_ref[...]
    forward(0)
    spread(1)
    narrow(0, gate_w)
    narrow(1, up_w)
    gate_up(0)
    forward(1)
    for k in range(1, planes):
        if k + 1 < planes:
            spread(k + 1)
        if k == 1:
            narrow(2, down_w)
        if k > 2:
            down(k - 1)
            issue(k - 1)
        elif k == 2:
            down(1)
            issue(1)
        gate_up(k)
        if k + 1 < planes:
            forward(k + 1)
    late = list(range(1, planes)) + [0]
    down(0)
    if planes > 2:
        reduce_one(1)
    down(planes - 1)
    issue(planes - 1)
    issue(0)
    if planes == 2:
        reduce_one(1)
    for at in range(1, planes):
        reduce_one(late[at])
        reduce_two(late[at - 1])
    reduce_two(0)

    total = own_sum[...]
    for k in range(1, planes):
        arrived("zs", k)
        total = total + z_recv[k].astype(F32)
    stream = 0.1 * x_ref[...].astype(F32) + total * down_scale_ref[...]
    own_sum[...] = stream
    last_send[...] = jnp.broadcast_to(
        jnp.sum(stream * stream, axis=1, keepdims=True), last_send.shape
    )
    send("last", 0, last_send, last_recv, core_peer)
    arrived("last", 0)
    both = (last_send[...] + last_recv[...])[:, :1]
    rscale = lax.rsqrt(both / features + EPS)
    out_ref[...] = (own_sum[...] * rscale * gain2_ref[...]).astype(BF16)
    for copy in copies.values():
        copy.wait_send()


def fused(
    planes,
    activations,
    gain_first,
    gate_weight,
    gate_scale,
    up_weight,
    up_scale,
    down_weight,
    down_scale,
    gain_second,
):
    rows, width = activations.shape
    units = gate_weight.shape[0]
    half = width // 2
    group = 4 * rows
    n_copies = 20 * planes
    vmem = pl.BlockSpec(memory_space=pltpu.VMEM)
    hbm = pl.BlockSpec(memory_space=pl.ANY)
    scratch = [
        pltpu.VMEM((3, units, width), F32),
        pltpu.VMEM((units, width), BF16),
        pltpu.VMEM((units, width), BF16),
        pltpu.VMEM((units, width), BF16),
        pltpu.VMEM((planes, 4, rows, width), BF16),
        pltpu.VMEM((4, rows, width), BF16),
        pltpu.VMEM((group, units), BF16),
        pltpu.VMEM((planes, 2, group, units), F32),
        pltpu.VMEM((planes, 2, group, units), BF16),
        pltpu.VMEM((planes, 2, group, units), BF16),
        pltpu.VMEM((planes, 4, rows, 128), F32),
        pltpu.VMEM((planes, 4, rows, 128), F32),
        pltpu.VMEM((planes, 2, rows, half), F32),
        pltpu.VMEM((planes, 2, rows, half), F32),
        pltpu.VMEM((planes, 2, rows, half), BF16),
        pltpu.VMEM((planes, 2, rows, half), BF16),
        pltpu.VMEM((planes, 2, rows, half), BF16),
        pltpu.VMEM((planes, 2, rows, half), BF16),
        pltpu.VMEM((planes, rows, half), BF16),
        pltpu.VMEM((planes, rows, half), BF16),
        pltpu.VMEM((planes, rows, half), BF16),
        pltpu.VMEM((planes, rows, half), BF16),
        pltpu.VMEM((rows, width), F32),
        pltpu.VMEM((planes, rows, width), BF16),
        pltpu.VMEM((planes, rows, width), BF16),
        pltpu.VMEM((rows, 128), F32),
        pltpu.VMEM((rows, 128), F32),
        pltpu.SemaphoreType.DMA((3,)),
        pltpu.SemaphoreType.DMA((n_copies,)),
        pltpu.SemaphoreType.DMA((n_copies,)),
    ]
    return pl.pallas_call(
        functools.partial(kernel, planes, width * 2),
        out_shape=jax.ShapeDtypeStruct((rows, width), BF16),
        in_specs=[vmem, vmem, hbm, vmem, hbm, vmem, hbm, vmem, vmem],
        out_specs=vmem,
        scratch_shapes=scratch,
        compiler_params=pltpu.CompilerParams(
            collective_id=0, has_side_effects=True, vmem_limit_bytes=60 * 1024 * 1024
        ),
    )(
        activations,
        gain_first[None, :],
        gate_weight,
        gate_scale,
        up_weight,
        up_scale,
        down_weight,
        down_scale[None, :],
        gain_second[None, :],
    )


def plain(
    activations,
    gain_first,
    gate_weight,
    gate_scale,
    up_weight,
    up_scale,
    down_weight,
    down_scale,
    gain_second,
):
    inputs = activations.astype(F32)
    features = activations.shape[1] * lax.axis_size("cb")
    gate_local = gate_weight.astype(BF16)
    up_local = up_weight.astype(BF16)
    down_local = down_weight.astype(BF16)
    gathered = lax.all_gather(activations, "ra", axis=0, tiled=True)
    wide_rows = gathered.astype(F32)
    row_squares = jnp.sum(wide_rows * wide_rows, axis=1)
    scaled = (wide_rows * gain_first).astype(BF16)
    contract = (((1,), (1,)), ((), ()))
    squares = lax.psum(row_squares, "cb")
    gate_part = lax.dot_general(gate_local, scaled, contract, preferred_element_type=F32)
    up_part = lax.dot_general(up_local, scaled, contract, preferred_element_type=F32)
    gate_sum, up_sum = lax.psum((gate_part, up_part), "cb")
    rscale_first = lax.rsqrt(squares / features + EPS)[None, :]
    gate_full = gate_sum * rscale_first * gate_scale[:, None]
    up_full = up_sum * rscale_first * up_scale[:, None]
    hidden = (jax.nn.silu(gate_full) * up_full).astype(BF16)
    mixed = lax.dot_general(hidden, down_local, (((0,), (0,)), ((), ())), preferred_element_type=F32)
    summed = lax.psum_scatter(mixed, "ra", scatter_dimension=0, tiled=True)
    stream = 0.1 * inputs + summed * down_scale
    second = lax.psum(jnp.sum(stream * stream, axis=1), "cb")
    rscale_second = lax.rsqrt(second / features + EPS)[:, None]
    return (stream * rscale_second * gain_second).astype(BF16)


def solution(mesh):
    placed = (
        P("ra", "cb"),
        P("cb"),
        P("ra", "cb"),
        P("ra"),
        P("ra", "cb"),
        P("ra"),
        P("ra", "cb"),
        P("cb"),
        P("cb"),
    )
    planes = mesh.shape["ra"] // 4
    paired = mesh.shape["cb"] == 2 and planes >= 2 and planes & (planes - 1) == 0
    body = functools.partial(fused, planes) if paired else plain
    return jax.shard_map(
        body, mesh=mesh, in_specs=placed, out_specs=P("ra", "cb"), check_vma=False
    )
```

profile of v0, /device:TPU:1, one launch (start us, length us, event | category | flops | bytes accessed | tf_op | source)
XLA Modules:
  0.0 78.5 jit_solution(5321093766934675064)
XLA Ops:
  0.0 76.9 %shard_map.91 = bf16[48,2048]{1,0:T(8,128)(2,1)} custom-call(bf16[48,2048]{1,0:T(8,128)(2,1)} %x_ref.1, f32[1,2048]{1,0:T(1,128)} %bitcast.3, f32[704,2048]{1,0:T(8,128)} %gate_hbm.1, f32[704]{0:T(1024)} %gate_scale_ref.1, f32[704,2048]{1,0:T(8,128)} %up_hbm.1, f32[704]{0:T(1024)} %up_scale_ref.1, f32[704,2048]{1,0:T(8,128)} %down_hbm.1, f32[1,2048]{1,0:T(1,128)} %bitcast.4, ...), custom_call_target="tpu_custom_call" | custom-call | tf_op jit(solution)/shard_map/pallas_call | solution.py:320
  76.9 1.6 %copy.11 = bf16[48,2048]{1,0:T(8,128)(2,1)} copy(bf16[48,2048]{1,0:T(8,128)(2,1)} %shard_map.91) | data formatting | bytes 393216
where the time goes:
time: 80.1 us; the launch traced here: 78.5 us
  Pallas kernels  76.9 us (96%)
  local copies, waits for them, and re-layouts  1.62 us (2%)
    pallas_call x1, Pallas kernels, fused(): pl.pallas_call(functools.partial(kernel, planes, width * 2), out_shape=ja...  76.9 us
    unnamed x1, local copies, waits for them, and re-layouts  1.62 us

commit v1 on v0

v1 whole, which is shorter than its diff:
```python
import functools

import jax
import jax.numpy as jnp
from jax import lax
from jax.experimental import pallas as pl
from jax.experimental.pallas import tpu as pltpu
from jax.sharding import PartitionSpec as P

EPS = 1e-06
MESH = pl.DeviceIdType.MESH
F32 = jnp.float32
BF16 = jnp.bfloat16


def flip(index, mask):
    bit = 1
    while bit <= mask:
        if mask & bit:
            index = index + (1 - 2 * ((index // bit) % 2)) * bit
        bit *= 2
    return index


def kernel(
    planes,
    features,
    x_hbm,
    gain_hbm,
    gate_hbm,
    gate_scale_hbm,
    up_hbm,
    up_scale_hbm,
    down_hbm,
    down_scale_hbm,
    gain2_hbm,
    out_ref,
    wide,
    gate_w,
    up_w,
    down_w,
    gain_ref,
    gate_scale_ref,
    up_scale_ref,
    down_scale_ref,
    gain2_ref,
    xg,
    scaled,
    hidden,
    part,
    ex_send,
    ex_recv,
    sq_send,
    sq_recv,
    keep_a,
    keep_b,
    send_a,
    send_b,
    recv_a,
    recv_b,
    send2_a,
    send2_b,
    recv2_a,
    recv2_b,
    far,
    own_sum,
    z_send,
    z_recv,
    last_send,
    last_recv,
    in_sem,
    w_sem,
    ssem,
    rsem,
    zs_sem,
    zr_sem,
):
    ra = lax.axis_index("ra")
    cb = lax.axis_index("cb")
    rows, width = xg.shape[2:]
    half = width // 2
    x_peer = (flip(ra, 1), cb)
    y_peer = (flip(ra, 2), cb)
    z_peers = [None] + [(flip(ra, 4 * k), cb) for k in range(1, planes)]
    core_peer = (ra, flip(cb, 1))
    halves = (pl.ds(0, half), pl.ds(half, half))
    first, second = halves

    barrier = pltpu.get_barrier_semaphore()
    peers = [x_peer, y_peer, core_peer] + z_peers[1:]
    for peer in peers:
        pl.semaphore_signal(barrier, inc=1, device_id=peer, device_id_type=MESH)
    own = pltpu.make_async_copy(x_hbm, xg.at[0, 0], in_sem.at[0])
    own.start()
    small = []
    for i, (src, dst) in enumerate(
        (
            (gain_hbm, gain_ref),
            (gate_scale_hbm, gate_scale_ref),
            (up_scale_hbm, up_scale_ref),
            (down_scale_hbm, down_scale_ref),
            (gain2_hbm, gain2_ref),
        )
    ):
        load = pltpu.make_async_copy(src, dst, in_sem.at[i + 1])
        load.start()
        small.append(load)
    loads = []
    for i, src in enumerate((gate_hbm, up_hbm, down_hbm)):
        load = pltpu.make_async_copy(src, wide.at[i], w_sem.at[i])
        load.start()
        loads.append(load)
    own.wait()
    pl.semaphore_wait(barrier, len(peers))

    copies = {}
    slots = []

    def send(name, k, src, dst, peer):
        slot = len(slots)
        slots.append(name)
        copy = pltpu.make_async_remote_copy(
            src_ref=src,
            dst_ref=dst,
            send_sem=ssem.at[slot],
            recv_sem=rsem.at[slot],
            device_id=peer,
            device_id_type=MESH,
        )
        copy.start()
        copies[name, k] = copy

    seen = set()

    def arrived(name, k):
        if (name, k) in seen:
            return
        seen.add((name, k))
        copies[name, k].wait_recv()

    def to_x(k, h):
        send(("gx", h), k, xg.at[k, 0, :, halves[h]], xg.at[k, 1, :, halves[h]], x_peer)

    def to_y(k, h):
        send(("gy", h), k, xg.at[k, 0, :, halves[h]], xg.at[k, 2, :, halves[h]], y_peer)

    level = ra // 4
    inner = level % 2 != level // 2
    relays = []

    def to_z(source, target, h, peer):
        slot = len(relays)
        copy = pltpu.make_async_remote_copy(
            src_ref=xg.at[source, 0, :, halves[h]],
            dst_ref=xg.at[target, 0, :, halves[h]],
            send_sem=zs_sem.at[slot],
            recv_sem=zr_sem.at[target, h],
            device_id=z_peers[peer],
            device_id_type=MESH,
        )
        copies[("z", h), target] = copy
        relays.append(copy)
        if source or peer != 1:
            pl.when(inner)(copy.start)
        else:
            copy.start()

    def spread(k, h):
        to_x(k, h)
        to_y(k, h)

    def at_z1(h):
        arrived(("z", h), 1)
        to_z(1, 2, h, 3)

    def at_z2(h):
        arrived(("z", h), 2)
        to_z(2, 3, h, 1)
        spread(2, h)

    def relay_z3(h):
        @pl.when(inner)
        def _():
            copies[("z", h), 3].wait_recv()

        to_z(3, 2, h, 1)

    def at_z3(h):
        @pl.when(jnp.logical_not(inner))
        def _():
            copies[("z", h), 3].wait_recv()

        spread(3, h)

    def across(h):
        arrived(("fx", "fy")[h], 0)
        send(("e", h), 1, xg.at[0, 3, :, halves[h]], xg.at[1, 3, :, halves[h]], z_peers[1])

    def forward_y(k):
        arrived(("gx", 1), k)
        send("fy", k, xg.at[k, 1, :, second], xg.at[k, 3, :, second], y_peer)

    def forward_x(k):
        arrived(("gy", 0), k)
        send("fx", k, xg.at[k, 2, :, first], xg.at[k, 3, :, first], x_peer)

    nt = (((1,), (1,)), ((), ()))

    def prepare(k):
        def slot(s):
            block = xg[k, s].astype(F32)
            squares = jnp.sum(block * block, axis=1, keepdims=True)
            sq_send[k, s] = jnp.broadcast_to(squares, (rows, 128))
            scaled[s] = (block * gain_ref[...]).astype(BF16)

        slot(0)
        arrived(("gx", 1), k)
        arrived(("gx", 0), k)
        slot(1)
        arrived(("gy", 0), k)
        arrived(("gy", 1), k)
        slot(2)
        if k == 1:
            arrived(("e", 1), 1)
            arrived(("e", 0), 1)
        else:
            arrived("fy", k)
            if k == 0:
                across(1)
            arrived("fx", k)
            if k == 0:
                across(0)
        slot(3)
        send("sq", k, sq_send.at[k], sq_recv.at[k], core_peer)

    def product(k, i):
        tokens = scaled[...].reshape(4 * rows, width)
        w = (gate_w, up_w)[i]
        product = lax.dot_general(tokens, w[...], nt, preferred_element_type=F32)
        part[k, i] = product
        ex_send[k, i] = product.astype(BF16)
        send(("ex", i), k, ex_send.at[k, i], ex_recv.at[k, i], core_peer)

    def activate(k):
        arrived("sq", k)
        arrived(("ex", 0), k)
        arrived(("ex", 1), k)
        for s in range(4):
            here = slice(s * rows, (s + 1) * rows)
            squares = (sq_send[k, s] + sq_recv[k, s])[:, :1]
            rscale = lax.rsqrt(squares / features + EPS)
            gate = (part[k, 0, here] + ex_recv[k, 0, here].astype(F32)) * rscale * gate_scale_ref[...][None, :]
            up = (part[k, 1, here] + ex_recv[k, 1, here].astype(F32)) * rscale * up_scale_ref[...][None, :]
            hidden[k, here] = (gate / (1.0 + jnp.exp(-gate)) * up).astype(BF16)

    def down_a(k):
        prod = jnp.dot(hidden[k], down_w[:, :half], preferred_element_type=F32)
        keep_a[k, 0] = prod[:rows]
        send_a[k, 0] = prod[rows : 2 * rows].astype(BF16)
        if k == 1:
            send2_a[k] = prod[2 * rows : 3 * rows].astype(BF16)
        else:
            keep_a[k, 1] = prod[2 * rows : 3 * rows]
        if k:
            send_a[k, 1] = prod[3 * rows :].astype(BF16)
        else:
            far[0] = prod[3 * rows :]

    def down_b(k):
        prod = jnp.dot(hidden[k], down_w[:, half:], preferred_element_type=F32)
        keep_b[k, 0] = prod[:rows]
        if k == 1:
            send2_b[k] = prod[rows : 2 * rows].astype(BF16)
        else:
            keep_b[k, 1] = prod[rows : 2 * rows]
        send_b[k, 0] = prod[2 * rows : 3 * rows].astype(BF16)
        if k:
            send_b[k, 1] = prod[3 * rows :].astype(BF16)
        else:
            far[1] = prod[3 * rows :]

    def one_a(k, d):
        send(("a1", d), k, send_a.at[k, d], recv_a.at[k, d], x_peer)

    def one_b(k, d):
        send(("b1", d), k, send_b.at[k, d], recv_b.at[k, d], y_peer)

    def down(k):
        activate(k)
        down_a(k)
        if k == 1:
            send(("r", 0), 1, send_a.at[1, 1], recv_a.at[1, 1], z_peers[1])
            one_a(1, 0)
            send("a2", 1, send2_a.at[1], recv2_a.at[1], y_peer)
        else:
            one_a(k, 1)
        down_b(k)
        if k == 1:
            send(("r", 1), 1, send_b.at[1, 1], recv_b.at[1, 1], z_peers[1])
            one_b(1, 0)
            send("b2", 1, send2_b.at[1], recv2_b.at[1], x_peer)
        else:
            one_b(k, 1)
            one_a(k, 0)
            one_b(k, 0)

    def merge():
        arrived(("r", 0), 1)
        send_a[0, 1] = (far[0] + recv_a[1, 1].astype(F32)).astype(BF16)
        one_a(0, 1)
        arrived(("r", 1), 1)
        send_b[0, 1] = (far[1] + recv_b[1, 1].astype(F32)).astype(BF16)
        one_b(0, 1)

    def two(k):
        arrived(("a1", 1), k)
        send2_a[k] = (keep_a[k, 1] + recv_a[k, 1].astype(F32)).astype(BF16)
        send("a2", k, send2_a.at[k], recv2_a.at[k], y_peer)
        arrived(("b1", 1), k)
        send2_b[k] = (keep_b[k, 1] + recv_b[k, 1].astype(F32)).astype(BF16)
        send("b2", k, send2_b.at[k], recv2_b.at[k], x_peer)

    def home(k):
        arrived(("a1", 0), k)
        arrived("a2", k)
        sum_a = keep_a[k, 0] + recv_a[k, 0].astype(F32) + recv2_a[k].astype(F32)
        if k:
            z_send[k, 0] = sum_a.astype(BF16)
            send(("zs", 0), k, z_send.at[k, 0], z_recv.at[k, 0], z_peers[k])
        arrived(("b1", 0), k)
        arrived("b2", k)
        sum_b = keep_b[k, 0] + recv_b[k, 0].astype(F32) + recv2_b[k].astype(F32)
        if k:
            z_send[k, 1] = sum_b.astype(BF16)
            send(("zs", 1), k, z_send.at[k, 1], z_recv.at[k, 1], z_peers[k])
            return
        own_sum[:, :half] = sum_a
        own_sum[:, half:] = sum_b

    def collect(k):
        for h in range(2):
            arrived(("zs", h), k)
            own_sum[:, halves[h]] += z_recv[k, h].astype(F32)

    def narrow(i, target):
        loads[i].wait()
        step = 64

        def body(j, carry):
            here = pl.ds(pl.multiple_of(j * step, step), step)
            target[here] = wide[i, here].astype(BF16)
            return carry

        lax.fori_loop(0, target.shape[0] // step, body, 0)

    for h in (1, 0):
        to_x(0, h)
        to_y(0, 1 - h)
        to_z(0, 1, h, 1)
    for h in (1, 0):
        to_z(0, 3, h, 3)
    narrow(0, gate_w)
    narrow(1, up_w)
    forward_y(0)
    forward_x(0)
    for h in (1, 0):
        relay_z3(h)
        at_z1(h)
        spread(1, h)
    for load in small:
        load.wait()
    prepare(0)
    at_z2(1)
    product(0, 0)
    at_z2(0)
    product(0, 1)
    at_z3(1)
    forward_y(2)
    at_z3(0)
    forward_x(2)

    narrow(2, down_w)
    activate(0)
    down_a(0)
    down_b(0)
    forward_y(3)

    prepare(2)
    forward_x(3)
    one_a(0, 0)
    one_b(0, 0)
    product(2, 0)
    product(2, 1)
    prepare(3)
    product(3, 0)
    down(2)
    product(3, 1)
    prepare(1)
    product(1, 0)
    two(2)
    down(3)
    product(1, 1)
    home(2)
    two(3)
    down(1)
    home(3)
    merge()
    home(1)
    two(0)
    home(0)
    collect(2)
    collect(1)
    collect(3)

    stream = 0.1 * xg[0, 0].astype(F32) + own_sum[...] * down_scale_ref[...]
    own_sum[...] = stream
    last_send[...] = jnp.broadcast_to(
        jnp.sum(stream * stream, axis=1, keepdims=True), last_send.shape
    )
    send("last", 0, last_send, last_recv, core_peer)
    arrived("last", 0)
    both = (last_send[...] + last_recv[...])[:, :1]
    rscale = lax.rsqrt(both / features + EPS)
    out_ref[...] = (own_sum[...] * rscale * gain2_ref[...]).astype(BF16)
    for (name, _), copy in copies.items():
        if name[0] != "z":
            copy.wait_send()
    for copy in relays[:2]:
        copy.wait_send()

    @pl.when(inner)
    def _():
        for copy in relays[2:]:
            copy.wait_send()


def fused(
    planes,
    activations,
    gain_first,
    gate_weight,
    gate_scale,
    up_weight,
    up_scale,
    down_weight,
    down_scale,
    gain_second,
):
    rows, width = activations.shape
    units = gate_weight.shape[0]
    half = width // 2
    group = 4 * rows
    n_copies = 24 * planes
    vmem = pl.BlockSpec(memory_space=pltpu.VMEM)
    hbm = pl.BlockSpec(memory_space=pl.ANY)
    scratch = [
        pltpu.VMEM((3, units, width), F32),
        pltpu.VMEM((units, width), BF16),
        pltpu.VMEM((units, width), BF16),
        pltpu.VMEM((units, width), BF16),
        pltpu.VMEM((1, width), F32),
        pltpu.VMEM((units,), F32),
        pltpu.VMEM((units,), F32),
        pltpu.VMEM((1, width), F32),
        pltpu.VMEM((1, width), F32),
        pltpu.VMEM((planes, 4, rows, width), BF16),
        pltpu.VMEM((4, rows, width), BF16),
        pltpu.VMEM((planes, group, units), BF16),
        pltpu.VMEM((planes, 2, group, units), F32),
        pltpu.VMEM((planes, 2, group, units), BF16),
        pltpu.VMEM((planes, 2, group, units), BF16),
        pltpu.VMEM((planes, 4, rows, 128), F32),
        pltpu.VMEM((planes, 4, rows, 128), F32),
        pltpu.VMEM((planes, 2, rows, half), F32),
        pltpu.VMEM((planes, 2, rows, half), F32),
        pltpu.VMEM((planes, 2, rows, half), BF16),
        pltpu.VMEM((planes, 2, rows, half), BF16),
        pltpu.VMEM((planes, 2, rows, half), BF16),
        pltpu.VMEM((planes, 2, rows, half), BF16),
        pltpu.VMEM((planes, rows, half), BF16),
        pltpu.VMEM((planes, rows, half), BF16),
        pltpu.VMEM((planes, rows, half), BF16),
        pltpu.VMEM((planes, rows, half), BF16),
        pltpu.VMEM((2, rows, half), F32),
        pltpu.VMEM((rows, width), F32),
        pltpu.VMEM((planes, 2, rows, half), BF16),
        pltpu.VMEM((planes, 2, rows, half), BF16),
        pltpu.VMEM((rows, 128), F32),
        pltpu.VMEM((rows, 128), F32),
        pltpu.SemaphoreType.DMA((6,)),
        pltpu.SemaphoreType.DMA((3,)),
        pltpu.SemaphoreType.DMA((n_copies,)),
        pltpu.SemaphoreType.DMA((n_copies,)),
        pltpu.SemaphoreType.DMA((10,)),
        pltpu.SemaphoreType.DMA((planes, 2)),
    ]
    return pl.pallas_call(
        functools.partial(kernel, planes, width * 2),
        out_shape=jax.ShapeDtypeStruct((rows, width), BF16),
        in_specs=[hbm] * 9,
        out_specs=vmem,
        scratch_shapes=scratch,
        compiler_params=pltpu.CompilerParams(
            collective_id=0, has_side_effects=True, vmem_limit_bytes=60 * 1024 * 1024
        ),
    )(
        activations,
        gain_first[None, :],
        gate_weight,
        gate_scale,
        up_weight,
        up_scale,
        down_weight,
        down_scale[None, :],
        gain_second[None, :],
    )


def plain(
    activations,
    gain_first,
    gate_weight,
    gate_scale,
    up_weight,
    up_scale,
    down_weight,
    down_scale,
    gain_second,
):
    inputs = activations.astype(F32)
    features = activations.shape[1] * lax.axis_size("cb")
    gate_local = gate_weight.astype(BF16)
    up_local = up_weight.astype(BF16)
    down_local = down_weight.astype(BF16)
    gathered = lax.all_gather(activations, "ra", axis=0, tiled=True)
    wide_rows = gathered.astype(F32)
    row_squares = jnp.sum(wide_rows * wide_rows, axis=1)
    scaled = (wide_rows * gain_first).astype(BF16)
    contract = (((1,), (1,)), ((), ()))
    squares = lax.psum(row_squares, "cb")
    gate_part = lax.dot_general(gate_local, scaled, contract, preferred_element_type=F32)
    up_part = lax.dot_general(up_local, scaled, contract, preferred_element_type=F32)
    gate_sum, up_sum = lax.psum((gate_part, up_part), "cb")
    rscale_first = lax.rsqrt(squares / features + EPS)[None, :]
    gate_full = gate_sum * rscale_first * gate_scale[:, None]
    up_full = up_sum * rscale_first * up_scale[:, None]
    hidden = (jax.nn.silu(gate_full) * up_full).astype(BF16)
    mixed = lax.dot_general(hidden, down_local, (((0,), (0,)), ((), ())), preferred_element_type=F32)
    summed = lax.psum_scatter(mixed, "ra", scatter_dimension=0, tiled=True)
    stream = 0.1 * inputs + summed * down_scale
    second = lax.psum(jnp.sum(stream * stream, axis=1), "cb")
    rscale_second = lax.rsqrt(second / features + EPS)[:, None]
    return (stream * rscale_second * gain_second).astype(BF16)


def solution(mesh):
    placed = (
        P("ra", "cb"),
        P("cb"),
        P("ra", "cb"),
        P("ra"),
        P("ra", "cb"),
        P("ra"),
        P("ra", "cb"),
        P("cb"),
        P("cb"),
    )
    planes = mesh.shape["ra"] // 4
    paired = mesh.shape["cb"] == 2 and planes == 4
    body = functools.partial(fused, planes) if paired else plain
    return jax.shard_map(
        body, mesh=mesh, in_specs=placed, out_specs=P("ra", "cb"), check_vma=False
    )
```

time: 80.1 us -> 68.3 us (0.85); the launches traced: 78.5 us -> 68 us
  Pallas kernels: 76.9 us -> 66.3 us
    pallas_call x1, Pallas kernels: 76.9 us -> 66.3 us  [fused(): pl.pallas_call(functools.partial(kernel, planes, width * 2), out_shape=ja...]
where the time goes in v1:
time: 68.3 us; the launch traced here: 68 us
  Pallas kernels  66.3 us (97%)
  local copies, waits for them, and re-layouts  1.62 us (2%)
    pallas_call x1, Pallas kernels, fused(): pl.pallas_call(functools.partial(kernel, planes, width * 2), out_shape=ja...  66.3 us
    unnamed x1, local copies, waits for them, and re-layouts  1.62 us

profile of v1, /device:TPU:1, one launch (start us, length us, event | category | flops | bytes accessed | tf_op | source)
XLA Modules:
  0.0 68.0 jit_solution(13027228504052860243)
XLA Ops:
  0.0 66.3 %shard_map.91 = bf16[48,2048]{1,0:T(8,128)(2,1)} custom-call(bf16[48,2048]{1,0:T(8,128)(2,1)} %x_hbm.1, f32[1,2048]{1,0:T(1,128)} %bitcast.3, f32[704,2048]{1,0:T(8,128)} %gate_hbm.1, f32[704]{0:T(1024)} %gate_scale_hbm.1, f32[704,2048]{1,0:T(8,128)} %up_hbm.1, f32[704]{0:T(1024)} %up_scale_hbm.1, f32[704,2048]{1,0:T(8,128)} %down_hbm.1, f32[1,2048]{1,0:T(1,128)} %bitcast.4, ...), custom_call_target="tpu_custom_call" | custom-call | tf_op jit(solution)/shard_map/pallas_call | solution.py:497
  66.3 1.6 %copy.11 = bf16[48,2048]{1,0:T(8,128)(2,1)} copy(bf16[48,2048]{1,0:T(8,128)(2,1)} %shard_map.91) | data formatting | bytes 393216

commit v2 on v1

--- a/solution.py
+++ b/solution.py
@@ -192,10 +192,6 @@
 
         spread(3, h)
 
-    def across(h):
-        arrived(("fx", "fy")[h], 0)
-        send(("e", h), 1, xg.at[0, 3, :, halves[h]], xg.at[1, 3, :, halves[h]], z_peers[1])
-
     def forward_y(k):
         arrived(("gx", 1), k)
         send("fy", k, xg.at[k, 1, :, second], xg.at[k, 3, :, second], y_peer)
@@ -211,7 +207,7 @@
             block = xg[k, s].astype(F32)
             squares = jnp.sum(block * block, axis=1, keepdims=True)
             sq_send[k, s] = jnp.broadcast_to(squares, (rows, 128))
-            scaled[s] = (block * gain_ref[...]).astype(BF16)
+            scaled[k, s] = (block * gain_ref[...]).astype(BF16)
 
         slot(0)
         arrived(("gx", 1), k)
@@ -220,21 +216,13 @@
         arrived(("gy", 0), k)
         arrived(("gy", 1), k)
         slot(2)
-        if k == 1:
-            arrived(("e", 1), 1)
-            arrived(("e", 0), 1)
-        else:
-            arrived("fy", k)
-            if k == 0:
-                across(1)
-            arrived("fx", k)
-            if k == 0:
-                across(0)
+        arrived("fy", k)
+        arrived("fx", k)
         slot(3)
         send("sq", k, sq_send.at[k], sq_recv.at[k], core_peer)
 
     def product(k, i):
-        tokens = scaled[...].reshape(4 * rows, width)
+        tokens = scaled[k].reshape(4 * rows, width)
         w = (gate_w, up_w)[i]
         product = lax.dot_general(tokens, w[...], nt, preferred_element_type=F32)
         part[k, i] = product
@@ -269,11 +257,11 @@
     def down_b(k):
         prod = jnp.dot(hidden[k], down_w[:, half:], preferred_element_type=F32)
         keep_b[k, 0] = prod[:rows]
+        send_b[k, 0] = prod[2 * rows : 3 * rows].astype(BF16)
         if k == 1:
             send2_b[k] = prod[rows : 2 * rows].astype(BF16)
         else:
             keep_b[k, 1] = prod[rows : 2 * rows]
-        send_b[k, 0] = prod[2 * rows : 3 * rows].astype(BF16)
         if k:
             send_b[k, 1] = prod[3 * rows :].astype(BF16)
         else:
@@ -285,57 +273,56 @@
     def one_b(k, d):
         send(("b1", d), k, send_b.at[k, d], recv_b.at[k, d], y_peer)
 
-    def down(k):
-        activate(k)
-        down_a(k)
-        if k == 1:
-            send(("r", 0), 1, send_a.at[1, 1], recv_a.at[1, 1], z_peers[1])
-            one_a(1, 0)
-            send("a2", 1, send2_a.at[1], recv2_a.at[1], y_peer)
-        else:
-            one_a(k, 1)
-        down_b(k)
-        if k == 1:
-            send(("r", 1), 1, send_b.at[1, 1], recv_b.at[1, 1], z_peers[1])
-            one_b(1, 0)
-            send("b2", 1, send2_b.at[1], recv2_b.at[1], x_peer)
-        else:
-            one_b(k, 1)
-            one_a(k, 0)
-            one_b(k, 0)
-
-    def merge():
+    def cross_a():
+        send(("r", 0), 1, send_a.at[1, 1], recv_a.at[1, 1], z_peers[1])
+        one_a(1, 0)
+        send("a2", 1, send2_a.at[1], recv2_a.at[1], y_peer)
+
+    def cross_b():
+        send(("r", 1), 1, send_b.at[1, 1], recv_b.at[1, 1], z_peers[1])
+        one_b(1, 0)
+        send("b2", 1, send2_b.at[1], recv2_b.at[1], x_peer)
+
+    def merge_a():
         arrived(("r", 0), 1)
         send_a[0, 1] = (far[0] + recv_a[1, 1].astype(F32)).astype(BF16)
         one_a(0, 1)
+
+    def merge_b():
         arrived(("r", 1), 1)
         send_b[0, 1] = (far[1] + recv_b[1, 1].astype(F32)).astype(BF16)
         one_b(0, 1)
 
-    def two(k):
+    def two_a(k):
         arrived(("a1", 1), k)
         send2_a[k] = (keep_a[k, 1] + recv_a[k, 1].astype(F32)).astype(BF16)
         send("a2", k, send2_a.at[k], recv2_a.at[k], y_peer)
+
+    def two_b(k):
         arrived(("b1", 1), k)
         send2_b[k] = (keep_b[k, 1] + recv_b[k, 1].astype(F32)).astype(BF16)
         send("b2", k, send2_b.at[k], recv2_b.at[k], x_peer)
 
-    def home(k):
+    def home(k, h, mine):
+        if k == 0:
+            own_sum[:, halves[h]] = mine
+            return
+        if k == 3:
+            arrived(("zs", h), 2)
+            mine = mine + z_recv[2, h].astype(F32)
+        peer = z_peers[1 if k == 2 else k]
+        z_send[k, h] = mine.astype(BF16)
+        send(("zs", h), k, z_send.at[k, h], z_recv.at[k, h], peer)
+
+    def home_a(k):
         arrived(("a1", 0), k)
         arrived("a2", k)
-        sum_a = keep_a[k, 0] + recv_a[k, 0].astype(F32) + recv2_a[k].astype(F32)
-        if k:
-            z_send[k, 0] = sum_a.astype(BF16)
-            send(("zs", 0), k, z_send.at[k, 0], z_recv.at[k, 0], z_peers[k])
+        home(k, 0, keep_a[k, 0] + recv_a[k, 0].astype(F32) + recv2_a[k].astype(F32))
+
+    def home_b(k):
         arrived(("b1", 0), k)
         arrived("b2", k)
-        sum_b = keep_b[k, 0] + recv_b[k, 0].astype(F32) + recv2_b[k].astype(F32)
-        if k:
-            z_send[k, 1] = sum_b.astype(BF16)
-            send(("zs", 1), k, z_send.at[k, 1], z_recv.at[k, 1], z_peers[k])
-            return
-        own_sum[:, :half] = sum_a
-        own_sum[:, half:] = sum_b
+        home(k, 1, keep_b[k, 0] + recv_b[k, 0].astype(F32) + recv2_b[k].astype(F32))
 
     def collect(k):
         for h in range(2):
@@ -359,58 +346,83 @@
         to_z(0, 1, h, 1)
     for h in (1, 0):
         to_z(0, 3, h, 3)
+    forward_x(0)
+    forward_y(0)
+    relay_z3(1)
+    narrow(1, up_w)
     narrow(0, gate_w)
-    narrow(1, up_w)
-    forward_y(0)
-    forward_x(0)
-    for h in (1, 0):
-        relay_z3(h)
-        at_z1(h)
-        spread(1, h)
+    at_z1(1)
+    at_z1(0)
+    spread(1, 0)
+    relay_z3(0)
+    at_z2(1)
+    narrow(2, down_w)
+    at_z2(0)
     for load in small:
         load.wait()
     prepare(0)
-    at_z2(1)
-    product(0, 0)
-    at_z2(0)
     product(0, 1)
-    at_z3(1)
+    forward_x(2)
     forward_y(2)
     at_z3(0)
-    forward_x(2)
-
-    narrow(2, down_w)
+    at_z3(1)
+    product(0, 0)
+    prepare(2)
     activate(0)
+    spread(1, 1)
+    product(2, 1)
+    forward_x(3)
+    product(2, 0)
     down_a(0)
+    forward_y(3)
+    forward_x(1)
+    forward_y(1)
     down_b(0)
-    forward_y(3)
-
-    prepare(2)
-    forward_x(3)
+    activate(2)
+    down_b(2)
+    one_b(2, 0)
+    down_a(2)
+    one_a(2, 1)
+    one_a(2, 0)
+    prepare(3)
+    product(3, 1)
+    one_b(2, 1)
     one_a(0, 0)
+    product(3, 0)
+    prepare(1)
+    product(1, 1)
     one_b(0, 0)
-    product(2, 0)
-    product(2, 1)
-    prepare(3)
-    product(3, 0)
-    down(2)
-    product(3, 1)
-    prepare(1)
+    two_a(2)
     product(1, 0)
-    two(2)
-    down(3)
-    product(1, 1)
-    home(2)
-    two(3)
-    down(1)
-    home(3)
-    merge()
-    home(1)
-    two(0)
-    home(0)
-    collect(2)
+    activate(3)
+    down_a(3)
+    one_a(3, 1)
+    down_b(3)
+    one_b(3, 1)
+    two_b(2)
+    activate(1)
+    one_a(3, 0)
+    home_a(2)
+    down_a(1)
+    cross_a()
+    two_a(3)
+    down_b(1)
+    two_b(3)
+    one_b(3, 0)
+    cross_b()
+    home_b(2)
+    home_a(1)
+    home_a(3)
+    merge_b()
+    merge_a()
+    home_b(3)
+    home_b(1)
+    two_a(0)
+    two_b(0)
+    home_b(0)
+    home_a(0)
+    collect(3)
     collect(1)
-    collect(3)
 
     stream = 0.1 * xg[0, 0].astype(F32) + own_sum[...] * down_scale_ref[...]
     own_sum[...] = stream
@@ -464,7 +476,7 @@
         pltpu.VMEM((1, width), F32),
         pltpu.VMEM((1, width), F32),
         pltpu.VMEM((planes, 4, rows, width), BF16),
-        pltpu.VMEM((4, rows, width), BF16),
+        pltpu.VMEM((planes, 4, rows, width), BF16),
         pltpu.VMEM((planes, group, units), BF16),
         pltpu.VMEM((planes, 2, group, units), F32),
         pltpu.VMEM((planes, 2, group, units), BF16),
@@ -496,7 +508,7 @@
     ]
     return pl.pallas_call(
         functools.partial(kernel, planes, width * 2),
-        out_shape=jax.ShapeDtypeStruct((rows, width), BF16),
+        out_shape=pltpu.VMEM((rows, width), BF16),
         in_specs=[hbm] * 9,
         out_specs=vmem,
         scratch_shapes=scratch,

time: 68.3 us -> 63.3 us (0.927)
  Pallas kernels: 66.3 us -> 62.5 us
  local copies, waits for them, and re-layouts: 1.62 us -> 0.68 us
    pallas_call x1, Pallas kernels: 66.3 us -> 62.5 us  [fused(): pl.pallas_call(functools.partial(kernel, planes, width * 2), out_shape=pl...]
    unnamed x1, local copies, waits for them, and re-layouts: 1.62 us -> 0.68 us
where the time goes in v2:
time: 63.3 us; the launch traced here: 63.1 us
  Pallas kernels  62.5 us (99%)
  local copies, waits for them, and re-layouts  0.68 us (1%)
    pallas_call x1, Pallas kernels, fused(): pl.pallas_call(functools.partial(kernel, planes, width * 2), out_shape=pl...  62.5 us

profile of v2, /device:TPU:1, one launch (start us, length us, event | category | flops | bytes accessed | tf_op | source)
XLA Modules:
  0.0 63.1 jit_solution(5317940593147525846)
XLA Ops:
  0.0 62.5 %shard_map.91 = bf16[48,2048]{1,0:T(8,128)(2,1)S(1)} custom-call(bf16[48,2048]{1,0:T(8,128)(2,1)} %x_hbm.1, f32[1,2048]{1,0:T(1,128)} %bitcast.3, f32[704,2048]{1,0:T(8,128)} %gate_hbm.1, f32[704]{0:T(1024)} %gate_scale_hbm.1, f32[704,2048]{1,0:T(8,128)} %up_hbm.1, f32[704]{0:T(1024)} %up_scale_hbm.1, f32[704,2048]{1,0:T(8,128)} %down_hbm.1, ...), custom_call_target="tpu_custom_call" | custom-call | tf_op jit(solution)/shard_map/pallas_call | solution.py:509
  62.5 0.7 %copy.11 = bf16[48,2048]{1,0:T(8,128)(2,1)} copy(bf16[48,2048]{1,0:T(8,128)(2,1)S(1)} %shard_map.91) | data formatting | bytes 393216

commit v3 on v2

--- a/solution.py
+++ b/solution.py
@@ -115,14 +115,18 @@
 
     copies = {}
     slots = []
+    landed = {}
+    idle = []
+    early = list(range(ssem.shape[0]))
 
     def send(name, k, src, dst, peer):
         slot = len(slots)
         slots.append(name)
+        landed[name, k] = rsem.at[slot]
         copy = pltpu.make_async_remote_copy(
             src_ref=src,
             dst_ref=dst,
-            send_sem=ssem.at[slot],
+            send_sem=idle.pop(0) if idle else ssem.at[early.pop(0)],
             recv_sem=rsem.at[slot],
             device_id=peer,
             device_id_type=MESH,
@@ -137,6 +141,7 @@
             return
         seen.add((name, k))
         copies[name, k].wait_recv()
+        idle.append(landed[name, k])
 
     def to_x(k, h):
         send(("gx", h), k, xg.at[k, 0, :, halves[h]], xg.at[k, 1, :, halves[h]], x_peer)
@@ -159,6 +164,7 @@
             device_id_type=MESH,
         )
         copies[("z", h), target] = copy
+        landed[("z", h), target] = zr_sem.at[target, h]
         relays.append(copy)
         if source or peer != 1:
             pl.when(inner)(copy.start)
@@ -191,6 +197,10 @@
             copies[("z", h), 3].wait_recv()
 
         spread(3, h)
+
+    def across(h):
+        arrived(("fx", "fy")[h], 0)
+        send(("e", h), 1, xg.at[0, 3, :, halves[h]], xg.at[1, 3, :, halves[h]], z_peers[1])
 
     def forward_y(k):
         arrived(("gx", 1), k)
@@ -216,8 +226,12 @@
         arrived(("gy", 0), k)
         arrived(("gy", 1), k)
         slot(2)
-        arrived("fy", k)
-        arrived("fx", k)
+        if k == 1:
+            arrived(("e", 1), 1)
+            arrived(("e", 0), 1)
+        else:
+            arrived("fy", k)
+            arrived("fx", k)
         slot(3)
         send("sq", k, sq_send.at[k], sq_recv.at[k], core_peer)
 
@@ -346,81 +360,81 @@
         to_z(0, 1, h, 1)
     for h in (1, 0):
         to_z(0, 3, h, 3)
+    narrow(0, gate_w)
+    forward_y(0)
     forward_x(0)
-    forward_y(0)
     relay_z3(1)
-    narrow(1, up_w)
-    narrow(0, gate_w)
     at_z1(1)
     at_z1(0)
     spread(1, 0)
     relay_z3(0)
     at_z2(1)
-    narrow(2, down_w)
     at_z2(0)
+    across(1)
+    at_z3(1)
     for load in small:
         load.wait()
     prepare(0)
+    across(0)
+    narrow(1, up_w)
+    product(0, 0)
+    forward_y(2)
+    forward_x(2)
+    spread(1, 1)
     product(0, 1)
-    forward_x(2)
-    forward_y(2)
+    narrow(2, down_w)
+    activate(0)
+    down_a(0)
+    one_a(0, 0)
     at_z3(0)
-    at_z3(1)
-    product(0, 0)
     prepare(2)
-    activate(0)
-    spread(1, 1)
+    product(2, 0)
     product(2, 1)
+    prepare(1)
+    forward_y(3)
     forward_x(3)
-    product(2, 0)
-    down_a(0)
-    forward_y(3)
-    forward_x(1)
-    forward_y(1)
-    down_b(0)
+    product(1, 0)
     activate(2)
     down_b(2)
-    one_b(2, 0)
     down_a(2)
     one_a(2, 1)
+    one_b(2, 1)
+    one_b(2, 0)
     one_a(2, 0)
+    product(1, 1)
     prepare(3)
+    product(3, 0)
     product(3, 1)
-    one_b(2, 1)
-    one_a(0, 0)
-    product(3, 0)
-    prepare(1)
-    product(1, 1)
-    one_b(0, 0)
     two_a(2)
-    product(1, 0)
+    two_b(2)
+    activate(1)
+    down_a(1)
+    down_b(0)
+    cross_a()
+    down_b(1)
     activate(3)
     down_a(3)
-    one_a(3, 1)
     down_b(3)
     one_b(3, 1)
-    two_b(2)
-    activate(1)
+    one_a(3, 1)
+    cross_b()
+    home_b(2)
+    two_a(3)
     one_a(3, 0)
-    home_a(2)
-    down_a(1)
-    cross_a()
-    two_a(3)
-    down_b(1)
     two_b(3)
     one_b(3, 0)
-    cross_b()
-    home_b(2)
-    home_a(1)
-    home_a(3)
     merge_b()
     merge_a()
+    home_a(2)
+    home_b(1)
+    one_b(0, 0)
+    home_a(3)
     home_b(3)
-    home_b(1)
+    two_b(0)
     two_a(0)
-    two_b(0)
+    home_a(1)
+    home_a(0)
     home_b(0)
-    home_a(0)
     collect(3)
     collect(1)
 
@@ -462,7 +476,7 @@
     units = gate_weight.shape[0]
     half = width // 2
     group = 4 * rows
-    n_copies = 24 * planes
+    n_copies = 17 * planes - 1
     vmem = pl.BlockSpec(memory_space=pltpu.VMEM)
     hbm = pl.BlockSpec(memory_space=pl.ANY)
     scratch = [
@@ -501,7 +515,7 @@
         pltpu.VMEM((rows, 128), F32),
         pltpu.SemaphoreType.DMA((6,)),
         pltpu.SemaphoreType.DMA((3,)),
-        pltpu.SemaphoreType.DMA((n_copies,)),
+        pltpu.SemaphoreType.DMA((3 * planes,)),
         pltpu.SemaphoreType.DMA((n_copies,)),
         pltpu.SemaphoreType.DMA((10,)),
         pltpu.SemaphoreType.DMA((planes, 2)),

time: 63.3 us -> 60 us (0.948)
  Pallas kernels: 62.5 us -> 59.2 us
    pallas_call x1, Pallas kernels: 62.5 us -> 59.2 us  [fused(): pl.pallas_call(functools.partial(kernel, planes, width * 2), out_shape=pl...]
where the time goes in v3:
time: 60 us; the launch traced here: 59.9 us
  Pallas kernels  59.2 us (99%)
  local copies, waits for them, and re-layouts  0.68 us (1%)
    pallas_call x1, Pallas kernels, fused(): pl.pallas_call(functools.partial(kernel, planes, width * 2), out_shape=pl...  59.2 us

profile of v3, /device:TPU:1, one launch (start us, length us, event | category | flops | bytes accessed | tf_op | source)
XLA Modules:
  0.0 59.9 jit_solution(8355428996160976522)
XLA Ops:
  0.0 59.2 %shard_map.91 = bf16[48,2048]{1,0:T(8,128)(2,1)S(1)} custom-call(bf16[48,2048]{1,0:T(8,128)(2,1)} %x_hbm.1, f32[1,2048]{1,0:T(1,128)} %bitcast.3, f32[704,2048]{1,0:T(8,128)} %gate_hbm.1, f32[704]{0:T(1024)} %gate_scale_hbm.1, f32[704,2048]{1,0:T(8,128)} %up_hbm.1, f32[704]{0:T(1024)} %up_scale_hbm.1, f32[704,2048]{1,0:T(8,128)} %down_hbm.1, ...), custom_call_target="tpu_custom_call" | custom-call | tf_op jit(solution)/shard_map/pallas_call | solution.py:523
  59.2 0.7 %copy.11 = bf16[48,2048]{1,0:T(8,128)(2,1)} copy(bf16[48,2048]{1,0:T(8,128)(2,1)S(1)} %shard_map.91) | data formatting | bytes 393216

commit v4 on v3

--- a/solution.py
+++ b/solution.py
@@ -171,18 +171,13 @@
         else:
             copy.start()
 
-    def spread(k, h):
-        to_x(k, h)
-        to_y(k, h)
-
     def at_z1(h):
         arrived(("z", h), 1)
         to_z(1, 2, h, 3)
 
-    def at_z2(h):
+    def pass_z2(h):
         arrived(("z", h), 2)
         to_z(2, 3, h, 1)
-        spread(2, h)
 
     def relay_z3(h):
         @pl.when(inner)
@@ -191,13 +186,11 @@
 
         to_z(3, 2, h, 1)
 
-    def at_z3(h):
+    def wait_z3(h):
         @pl.when(jnp.logical_not(inner))
         def _():
             copies[("z", h), 3].wait_recv()
 
-        spread(3, h)
-
     def across(h):
         arrived(("fx", "fy")[h], 0)
         send(("e", h), 1, xg.at[0, 3, :, halves[h]], xg.at[1, 3, :, halves[h]], z_peers[1])
@@ -212,27 +205,22 @@
 
     nt = (((1,), (1,)), ((), ()))
 
-    def prepare(k):
-        def slot(s):
-            block = xg[k, s].astype(F32)
-            squares = jnp.sum(block * block, axis=1, keepdims=True)
-            sq_send[k, s] = jnp.broadcast_to(squares, (rows, 128))
-            scaled[k, s] = (block * gain_ref[...]).astype(BF16)
-
-        slot(0)
-        arrived(("gx", 1), k)
-        arrived(("gx", 0), k)
-        slot(1)
-        arrived(("gy", 0), k)
-        arrived(("gy", 1), k)
-        slot(2)
-        if k == 1:
-            arrived(("e", 1), 1)
-            arrived(("e", 0), 1)
-        else:
-            arrived("fy", k)
-            arrived("fx", k)
-        slot(3)
+    def slot(k, s):
+        if s == 1:
+            arrived(("gx", 1), k)
+            arrived(("gx", 0), k)
+        elif s == 2:
+            arrived(("gy", 0), k)
+            arrived(("gy", 1), k)
+        elif s == 3:
+            for h in (1, 0):
+                arrived(("e", h) if k == 1 else ("fx", "fy")[h], k)
+        block = xg[k, s].astype(F32)
+        total = jnp.sum(block * block, axis=1, keepdims=True)
+        sq_send[k, s] = jnp.broadcast_to(total, (rows, 128))
+        scaled[k, s] = (block * gain_ref[...]).astype(BF16)
+
+    def squares(k):
         send("sq", k, sq_send.at[k], sq_recv.at[k], core_peer)
 
     def product(k, i):
@@ -287,14 +275,14 @@
     def one_b(k, d):
         send(("b1", d), k, send_b.at[k, d], recv_b.at[k, d], y_peer)
 
-    def cross_a():
-        send(("r", 0), 1, send_a.at[1, 1], recv_a.at[1, 1], z_peers[1])
-        one_a(1, 0)
+    def send_r(h):
+        src, dst = ((send_a, recv_a), (send_b, recv_b))[h]
+        send(("r", h), 1, src.at[1, 1], dst.at[1, 1], z_peers[1])
+
+    def pass_a():
         send("a2", 1, send2_a.at[1], recv2_a.at[1], y_peer)
 
-    def cross_b():
-        send(("r", 1), 1, send_b.at[1, 1], recv_b.at[1, 1], z_peers[1])
-        one_b(1, 0)
+    def pass_b():
         send("b2", 1, send2_b.at[1], recv2_b.at[1], x_peer)
 
     def merge_a():
@@ -360,83 +348,113 @@
         to_z(0, 1, h, 1)
     for h in (1, 0):
         to_z(0, 3, h, 3)
-    narrow(0, gate_w)
-    forward_y(0)
-    forward_x(0)
     relay_z3(1)
     at_z1(1)
+    to_y(1, 1)
+    forward_x(0)
+    to_x(1, 1)
     at_z1(0)
-    spread(1, 0)
+    forward_y(0)
     relay_z3(0)
-    at_z2(1)
-    at_z2(0)
-    across(1)
-    at_z3(1)
     for load in small:
         load.wait()
-    prepare(0)
+    slot(0, 2)
+    narrow(0, gate_w)
+    pass_z2(1)
+    to_x(2, 1)
+    to_y(1, 0)
+    narrow(1, up_w)
+    to_x(1, 0)
+    narrow(2, down_w)
+    slot(0, 0)
+    pass_z2(0)
+    slot(0, 3)
+    to_y(2, 0)
+    slot(0, 1)
+    across(1)
     across(0)
-    narrow(1, up_w)
     product(0, 0)
+    wait_z3(1)
+    to_y(2, 1)
+    to_x(3, 1)
+    slot(1, 0)
+    slot(1, 2)
     forward_y(2)
+    to_x(2, 0)
     forward_x(2)
-    spread(1, 1)
+    slot(1, 1)
+    wait_z3(0)
+    to_y(3, 0)
+    slot(2, 0)
     product(0, 1)
-    narrow(2, down_w)
-    activate(0)
-    down_a(0)
-    one_a(0, 0)
-    at_z3(0)
-    prepare(2)
+    slot(1, 3)
+    product(1, 1)
+    slot(2, 1)
+    squares(1)
+    squares(0)
+    product(1, 0)
+    slot(2, 2)
+    to_y(3, 1)
+    to_x(3, 0)
+    forward_x(3)
+    slot(2, 3)
+    forward_y(3)
     product(2, 0)
+    squares(2)
     product(2, 1)
-    prepare(1)
-    forward_y(3)
-    forward_x(3)
-    product(1, 0)
+    activate(1)
+    down_a(1)
+    one_a(1, 0)
+    down_b(1)
+    pass_a()
     activate(2)
     down_b(2)
+    one_b(2, 1)
+    pass_b()
+    slot(3, 1)
     down_a(2)
+    slot(3, 0)
+    activate(0)
     one_a(2, 1)
-    one_b(2, 1)
+    send_r(1)
+    down_a(0)
+    slot(3, 2)
+    one_b(1, 0)
+    slot(3, 3)
+    one_a(2, 0)
     one_b(2, 0)
-    one_a(2, 0)
-    product(1, 1)
-    prepare(3)
+    squares(3)
+    send_r(0)
     product(3, 0)
     product(3, 1)
-    two_a(2)
+    home_a(1)
     two_b(2)
-    activate(1)
-    down_a(1)
-    down_b(0)
-    cross_a()
-    down_b(1)
     activate(3)
-    down_a(3)
     down_b(3)
     one_b(3, 1)
+    home_b(1)
+    two_a(2)
+    down_b(0)
+    down_a(3)
     one_a(3, 1)
-    cross_b()
     home_b(2)
-    two_a(3)
-    one_a(3, 0)
     two_b(3)
     one_b(3, 0)
+    one_a(3, 0)
+    two_a(3)
     merge_b()
+    one_b(0, 0)
     merge_a()
     home_a(2)
-    home_b(1)
-    one_b(0, 0)
+    one_a(0, 0)
+    home_b(3)
     home_a(3)
-    home_b(3)
     two_b(0)
     two_a(0)
-    home_a(1)
+    home_b(0)
     home_a(0)
-    home_b(0)
+    collect(1)
     collect(3)
-    collect(1)
 
     stream = 0.1 * xg[0, 0].astype(F32) + own_sum[...] * down_scale_ref[...]
     own_sum[...] = stream

time: 60 us -> 58.5 us (0.975)
  Pallas kernels: 59.2 us -> 57.6 us
    pallas_call x1, Pallas kernels: 59.2 us -> 57.6 us  [fused(): pl.pallas_call(functools.partial(kernel, planes, width * 2), out_shape=pl...]
where the time goes in v4:
time: 58.5 us; the launch traced here: 58.3 us
  Pallas kernels  57.6 us (98%)
  local copies, waits for them, and re-layouts  0.68 us (1%)
    pallas_call x1, Pallas kernels, fused(): pl.pallas_call(functools.partial(kernel, planes, width * 2), out_shape=pl...  57.6 us

profile of v4, /device:TPU:1, one launch (start us, length us, event | category | flops | bytes accessed | tf_op | source)
XLA Modules:
  0.0 58.3 jit_solution(11037411409612443109)
XLA Ops:
  0.0 57.6 %shard_map.91 = bf16[48,2048]{1,0:T(8,128)(2,1)S(1)} custom-call(bf16[48,2048]{1,0:T(8,128)(2,1)} %x_hbm.1, f32[1,2048]{1,0:T(1,128)} %bitcast.3, f32[704,2048]{1,0:T(8,128)} %gate_hbm.1, f32[704]{0:T(1024)} %gate_scale_hbm.1, f32[704,2048]{1,0:T(8,128)} %up_hbm.1, f32[704]{0:T(1024)} %up_scale_hbm.1, f32[704,2048]{1,0:T(8,128)} %down_hbm.1, ...), custom_call_target="tpu_custom_call" | custom-call | tf_op jit(solution)/shard_map/pallas_call | solution.py:541
  57.6 0.7 %copy.11 = bf16[48,2048]{1,0:T(8,128)(2,1)} copy(bf16[48,2048]{1,0:T(8,128)(2,1)S(1)} %shard_map.91) | data formatting | bytes 393216

commit v5 on v4

--- a/solution.py
+++ b/solution.py
@@ -350,109 +350,109 @@
         to_z(0, 3, h, 3)
     relay_z3(1)
     at_z1(1)
+    forward_y(0)
+    forward_x(0)
+    at_z1(0)
+    relay_z3(0)
+    to_y(1, 0)
+    to_x(1, 1)
     to_y(1, 1)
-    forward_x(0)
-    to_x(1, 1)
-    at_z1(0)
-    forward_y(0)
-    relay_z3(0)
     for load in small:
         load.wait()
+    slot(1, 0)
+    pass_z2(1)
+    to_x(2, 1)
+    slot(0, 3)
+    pass_z2(0)
+    to_y(2, 0)
+    to_x(1, 0)
+    slot(0, 0)
+    slot(0, 1)
+    to_y(2, 1)
+    to_x(2, 0)
     slot(0, 2)
     narrow(0, gate_w)
-    pass_z2(1)
-    to_x(2, 1)
-    to_y(1, 0)
+    across(0)
+    across(1)
+    forward_y(2)
+    wait_z3(1)
+    product(0, 0)
+    to_x(3, 1)
+    narrow(2, down_w)
     narrow(1, up_w)
-    to_x(1, 0)
-    narrow(2, down_w)
-    slot(0, 0)
-    pass_z2(0)
-    slot(0, 3)
-    to_y(2, 0)
-    slot(0, 1)
-    across(1)
-    across(0)
-    product(0, 0)
-    wait_z3(1)
-    to_y(2, 1)
-    to_x(3, 1)
-    slot(1, 0)
+    forward_x(2)
+    wait_z3(0)
     slot(1, 2)
-    forward_y(2)
-    to_x(2, 0)
-    forward_x(2)
+    to_y(3, 0)
+    squares(0)
+    product(0, 1)
     slot(1, 1)
-    wait_z3(0)
-    to_y(3, 0)
     slot(2, 0)
-    product(0, 1)
+    slot(2, 2)
+    slot(2, 1)
     slot(1, 3)
+    product(1, 0)
     product(1, 1)
-    slot(2, 1)
+    forward_x(3)
+    to_y(3, 1)
     squares(1)
-    squares(0)
-    product(1, 0)
-    slot(2, 2)
-    to_y(3, 1)
-    to_x(3, 0)
-    forward_x(3)
     slot(2, 3)
     forward_y(3)
+    squares(2)
+    to_x(3, 0)
     product(2, 0)
-    squares(2)
     product(2, 1)
     activate(1)
     down_a(1)
+    slot(3, 0)
     one_a(1, 0)
+    pass_a()
     down_b(1)
-    pass_a()
+    activate(0)
+    pass_b()
     activate(2)
+    down_a(2)
+    one_a(2, 0)
+    one_b(1, 0)
+    send_r(0)
     down_b(2)
-    one_b(2, 1)
-    pass_b()
-    slot(3, 1)
-    down_a(2)
-    slot(3, 0)
-    activate(0)
     one_a(2, 1)
     send_r(1)
-    down_a(0)
     slot(3, 2)
-    one_b(1, 0)
+    slot(3, 1)
     slot(3, 3)
-    one_a(2, 0)
+    one_b(2, 1)
     one_b(2, 0)
     squares(3)
-    send_r(0)
     product(3, 0)
     product(3, 1)
-    home_a(1)
-    two_b(2)
+    down_b(0)
+    down_a(0)
     activate(3)
     down_b(3)
     one_b(3, 1)
-    home_b(1)
-    two_a(2)
-    down_b(0)
+    two_b(2)
+    home_a(1)
     down_a(3)
     one_a(3, 1)
+    two_a(2)
+    home_b(1)
+    one_b(3, 0)
+    two_b(3)
+    one_a(3, 0)
     home_b(2)
-    two_b(3)
-    one_b(3, 0)
-    one_a(3, 0)
     two_a(3)
+    home_a(2)
     merge_b()
     one_b(0, 0)
     merge_a()
-    home_a(2)
     one_a(0, 0)
     home_b(3)
     home_a(3)
     two_b(0)
     two_a(0)
+    home_a(0)
     home_b(0)
-    home_a(0)
     collect(1)
     collect(3)
 

time: 58.5 us -> 57.9 us (0.990)
  no operation moved by 1% of the time
where the time goes in v5:
time: 57.9 us; the launch traced here: 57.8 us
  Pallas kernels  57.1 us (99%)
  local copies, waits for them, and re-layouts  0.68 us (1%)
    pallas_call x1, Pallas kernels, fused(): pl.pallas_call(functools.partial(kernel, planes, width * 2), out_shape=pl...  57.1 us

profile of v5, /device:TPU:1, one launch (start us, length us, event | category | flops | bytes accessed | tf_op | source)
XLA Modules:
  0.0 57.8 jit_solution(15122376118376094424)
XLA Ops:
  0.0 57.1 %shard_map.91 = bf16[48,2048]{1,0:T(8,128)(2,1)S(1)} custom-call(bf16[48,2048]{1,0:T(8,128)(2,1)} %x_hbm.1, f32[1,2048]{1,0:T(1,128)} %bitcast.3, f32[704,2048]{1,0:T(8,128)} %gate_hbm.1, f32[704]{0:T(1024)} %gate_scale_hbm.1, f32[704,2048]{1,0:T(8,128)} %up_hbm.1, f32[704]{0:T(1024)} %up_scale_hbm.1, f32[704,2048]{1,0:T(8,128)} %down_hbm.1, ...), custom_call_target="tpu_custom_call" | custom-call | tf_op jit(solution)/shard_map/pallas_call | solution.py:541
  57.1 0.7 %copy.11 = bf16[48,2048]{1,0:T(8,128)(2,1)} copy(bf16[48,2048]{1,0:T(8,128)(2,1)S(1)} %shard_map.91) | data formatting | bytes 393216

commit v6 on v4

--- a/solution.py
+++ b/solution.py
@@ -348,94 +348,93 @@
         to_z(0, 1, h, 1)
     for h in (1, 0):
         to_z(0, 3, h, 3)
-    relay_z3(1)
-    at_z1(1)
-    to_y(1, 1)
-    forward_x(0)
-    to_x(1, 1)
-    at_z1(0)
-    forward_y(0)
-    relay_z3(0)
     for load in small:
         load.wait()
-    slot(0, 2)
+    slot(0, 0)
+    narrow(1, up_w)
     narrow(0, gate_w)
+    at_z1(1)
+    forward_y(0)
+    forward_x(0)
+    relay_z3(1)
+    narrow(2, down_w)
+    at_z1(0)
+    to_y(1, 0)
+    to_y(1, 1)
+    relay_z3(0)
+    to_x(1, 0)
+    to_x(1, 1)
     pass_z2(1)
     to_x(2, 1)
-    to_y(1, 0)
-    narrow(1, up_w)
-    to_x(1, 0)
-    narrow(2, down_w)
-    slot(0, 0)
     pass_z2(0)
+    across(0)
     slot(0, 3)
+    slot(2, 0)
+    slot(0, 2)
     to_y(2, 0)
+    to_x(2, 0)
+    slot(1, 2)
+    to_y(2, 1)
     slot(0, 1)
+    wait_z3(1)
     across(1)
-    across(0)
+    to_x(3, 1)
     product(0, 0)
-    wait_z3(1)
-    to_y(2, 1)
-    to_x(3, 1)
+    forward_y(2)
+    wait_z3(0)
+    forward_x(2)
+    to_y(3, 0)
+    slot(1, 1)
     slot(1, 0)
-    slot(1, 2)
-    forward_y(2)
-    to_x(2, 0)
-    forward_x(2)
-    slot(1, 1)
-    wait_z3(0)
-    to_y(3, 0)
-    slot(2, 0)
     product(0, 1)
+    slot(2, 1)
+    slot(2, 2)
     slot(1, 3)
+    squares(1)
     product(1, 1)
-    slot(2, 1)
-    squares(1)
-    squares(0)
+    forward_y(3)
     product(1, 0)
-    slot(2, 2)
     to_y(3, 1)
     to_x(3, 0)
-    forward_x(3)
     slot(2, 3)
-    forward_y(3)
-    product(2, 0)
     squares(2)
     product(2, 1)
+    forward_x(3)
+    product(2, 0)
     activate(1)
     down_a(1)
+    squares(0)
+    pass_a()
     one_a(1, 0)
+    slot(3, 0)
     down_b(1)
-    pass_a()
+    pass_b()
     activate(2)
     down_b(2)
     one_b(2, 1)
-    pass_b()
     slot(3, 1)
+    send_r(1)
     down_a(2)
-    slot(3, 0)
-    activate(0)
     one_a(2, 1)
-    send_r(1)
-    down_a(0)
     slot(3, 2)
+    slot(3, 3)
+    product(3, 0)
     one_b(1, 0)
-    slot(3, 3)
-    one_a(2, 0)
     one_b(2, 0)
     squares(3)
     send_r(0)
-    product(3, 0)
     product(3, 1)
+    two_b(2)
+    one_a(2, 0)
+    activate(3)
     home_a(1)
-    two_b(2)
-    activate(3)
     down_b(3)
     one_b(3, 1)
+    down_a(3)
+    activate(0)
     home_b(1)
     two_a(2)
     down_b(0)
-    down_a(3)
     one_a(3, 1)
     home_b(2)
     two_b(3)
@@ -443,11 +442,12 @@
     one_a(3, 0)
     two_a(3)
     merge_b()
+    home_a(2)
+    down_a(0)
     one_b(0, 0)
     merge_a()
-    home_a(2)
+    home_b(3)
     one_a(0, 0)
-    home_b(3)
     home_a(3)
     two_b(0)
     two_a(0)

time: 58.5 us -> 58.4 us (level)
  no operation moved by 1% of the time
where the time goes in v6:
time: 58.4 us; the launch traced here: 58.2 us
  Pallas kernels  57.5 us (98%)
  local copies, waits for them, and re-layouts  0.68 us (1%)
    pallas_call x1, Pallas kernels, fused(): pl.pallas_call(functools.partial(kernel, planes, width * 2), out_shape=pl...  57.5 us

profile of v6, /device:TPU:1, one launch (start us, length us, event | category | flops | bytes accessed | tf_op | source)
XLA Modules:
  0.0 58.2 jit_solution(6490372749326580431)
XLA Ops:
  0.0 57.5 %shard_map.91 = bf16[48,2048]{1,0:T(8,128)(2,1)S(1)} custom-call(bf16[48,2048]{1,0:T(8,128)(2,1)} %x_hbm.1, f32[1,2048]{1,0:T(1,128)} %bitcast.3, f32[704,2048]{1,0:T(8,128)} %gate_hbm.1, f32[704]{0:T(1024)} %gate_scale_hbm.1, f32[704,2048]{1,0:T(8,128)} %up_hbm.1, f32[704]{0:T(1024)} %up_scale_hbm.1, f32[704,2048]{1,0:T(8,128)} %down_hbm.1, ...), custom_call_target="tpu_custom_call" | custom-call | tf_op jit(solution)/shard_map/pallas_call | solution.py:541
  57.6 0.7 %copy.11 = bf16[48,2048]{1,0:T(8,128)(2,1)} copy(bf16[48,2048]{1,0:T(8,128)(2,1)S(1)} %shard_map.91) | data formatting | bytes 393216
